TPU v7x, 256 devices: a whole 4x4x8 slice. The times are simulated.
256 devices in a mesh: ep: 16 (over y, x), tp: 16 (over z, core).
Axes of the slice: x: 4, y: 4, z: 8, core: 2. Of those that a mesh axis runs over, the one named last changes fastest.
Arguments:
- layer_in: bfloat16 [512, 2048], P('ep'), may hold values from -6 to 6
- attn_gain: float32 [2048], replicated, may hold values from 0.1 to 1.9
- query_weight: bfloat16 [2048, 1024], P(None, 'tp'), may hold values from -0.125 to 0.125
- key_weight: bfloat16 [2048, 1024], P(None, 'tp'), may hold values from -0.125 to 0.125
- value_weight: bfloat16 [2048, 1024], P(None, 'tp'), may hold values from -0.125 to 0.125
- forget_weight: bfloat16 [2048, 16], replicated, may hold values from -0.125 to 0.125
- forget_bias: float32 [16], replicated, may hold values from -2 to 3
- out_weight: bfloat16 [1024, 2048], P('tp'), may hold values from -0.1875 to 0.1875
- kv_cache: bfloat16 [512, 16, 1024, 128], P('ep', 'tp'), may hold values from -110 to 110
- cum_gates: float32 [512, 16, 1024], P('ep', 'tp'), may hold values from -144 to 0, as said below
- lengths: int32 [512], P('ep'), may hold values from 512 to 1024, as said below
- ffn_gain: float32 [2048], replicated, may hold values from 0.1 to 1.9
- route_ids: int32 [512, 6], P('ep'), may hold values from 0 to 127, all different within a row; in each aligned block of 32 rows (0 to 31, 32 to 63, ...) at most 2 rows name the same one
- route_weights: float32 [512, 6], P('ep'), may hold values from 0.1 to 1
- shared_gate: bfloat16 [2048, 512], P(None, 'tp'), may hold values from -0.125 to 0.125
- shared_up: bfloat16 [2048, 512], P(None, 'tp'), may hold values from -0.125 to 0.125
- shared_down: bfloat16 [512, 2048], P('tp'), may hold values from -0.25 to 0.25
- expert_gate: bfloat16 [256, 2048, 256], P(('ep', 'tp')), may hold values from -0.125 to 0.125
- expert_up: bfloat16 [256, 2048, 256], P(('ep', 'tp')), may hold values from -0.125 to 0.125
- expert_down: bfloat16 [256, 256, 2048], P(('ep', 'tp')), may hold values from -0.25 to 0.25
Outputs:
- layer_out: bfloat16 [512, 2048], P('ep')
- new_kv: bfloat16 [512, 16, 128], P('ep', 'tp')
Inputs may be any that keep to these rules, and one draw needn't show every extreme that they name: `cum_gates`: never rising along positions. `lengths`: every length is at most 1024, and some sequence's length is exactly 1024. `route_ids`: each row names 6 different experts. Among the 32 rows of one index of ep (aligned blocks), no expert is named by more than 2 rows, and in some block one expert is named by exactly 2 rows.
All inputs are finite; a program needn't handle non-finite values.
Results may differ from a plain program's by a relative error of at most 0.019.
Values may be sent and summed in bfloat16 or wider, within the bound.
No kernel may reach another device: no remote copies, remote signals or barrier semaphores. Data moves between devices by JAX's collectives and lax.ppermute only.
A program may use at most 64 MiB of HBM per device.

v0:
```python
import jax
import jax.numpy as jnp
from jax import lax
from jax.sharding import PartitionSpec as P

NORM_EPS = 1e-06


def cut_along(shard, dim, peers):
    before, after = (shard.shape[:dim], shard.shape[dim + 1 :])
    return jnp.moveaxis(shard.reshape(*before, peers, -1, *after), dim, 0)


def summed_on_arrival(shard, axis, dim):
    tiles = cut_along(shard, dim, lax.axis_size(axis))
    arrived = lax.all_to_all(tiles, axis, split_axis=0, concat_axis=0, tiled=True)
    return arrived.astype(jnp.float32).sum(axis=0)


def in_one_piece(arrays, axis, dim, along):
    both = jnp.concatenate(arrays, axis=along)
    filled, at, outs = (lax.all_gather(both, axis, axis=dim, tiled=True), 0, [])
    for a in arrays:
        outs.append(lax.slice_in_dim(filled, at, at + a.shape[along], axis=along))
        at += a.shape[along]
    return tuple(outs)


def rms_scale(stream, gain):
    wide = stream.astype(jnp.float32)
    factor = lax.rsqrt(jnp.mean(wide * wide, axis=-1, keepdims=True) + NORM_EPS)
    return (wide * factor * gain).astype(jnp.bfloat16)


def project(normed, weight):
    return jnp.dot(normed, weight, preferred_element_type=jnp.float32).astype(jnp.bfloat16)


def attend(queries, new_key, new_value, forget, kv_block, cum_block, length_block):
    head_size = queries.shape[-1]
    cache_span = kv_block.shape[2]
    positions = jnp.arange(cache_span, dtype=jnp.int32)
    inside = positions[None, None, :] < length_block[:, None, None]
    at_last = positions[None, None, :] == (length_block - 1)[:, None, None]
    latest = jnp.sum(jnp.where(at_last, cum_block, 0.0), axis=-1)
    scaling = head_size ** (-0.5)
    cached_keys = kv_block[..., :head_size]
    cached_values = kv_block[..., head_size:]
    scores = (
        jnp.einsum("shd,shld->shl", queries, cached_keys, preferred_element_type=jnp.float32)
        * scaling
    )
    scores = jnp.where(inside, scores + (latest + forget)[..., None] - cum_block, -jnp.inf)
    itself = jnp.sum(queries.astype(jnp.float32) * new_key.astype(jnp.float32), axis=-1) * scaling
    highest = jnp.maximum(jnp.max(scores, axis=-1), itself)
    earlier = jnp.exp(scores - highest[..., None])
    own_term = jnp.exp(itself - highest)
    denominator = jnp.sum(earlier, axis=-1) + own_term
    past_probs = (earlier / denominator[..., None]).astype(jnp.bfloat16)
    own_probs = (own_term / denominator).astype(jnp.bfloat16)
    blended = jnp.einsum(
        "shl,shld->shd", past_probs, cached_values, preferred_element_type=jnp.float32
    )
    blended = blended + own_probs.astype(jnp.float32)[..., None] * new_value.astype(jnp.float32)
    return blended.astype(jnp.bfloat16)


def body(
    layer_in,
    attn_gain,
    query_weight,
    key_weight,
    value_weight,
    forget_weight,
    forget_bias,
    out_weight,
    kv_cache,
    cum_gates,
    lengths,
    ffn_gain,
    route_ids,
    route_weights,
    shared_gate,
    shared_up,
    shared_down,
    expert_gate,
    expert_up,
    expert_down,
):
    row_count = layer_in.shape[0]
    width = layer_in.shape[1]
    heads_here = kv_cache.shape[1]
    head_size = kv_cache.shape[3] // 2
    normed = rms_scale(layer_in, attn_gain)
    queries = project(normed, query_weight).reshape(row_count, heads_here, head_size)
    new_key = project(normed, key_weight).reshape(row_count, heads_here, head_size)
    new_value = project(normed, value_weight).reshape(row_count, heads_here, head_size)
    new_kv = jnp.concatenate([new_key, new_value], axis=-1)
    first_head = lax.axis_index("tp") * heads_here
    gate_logits = jnp.dot(normed, forget_weight, preferred_element_type=jnp.float32) + forget_bias
    forget = jax.nn.log_sigmoid(lax.dynamic_slice_in_dim(gate_logits, first_head, heads_here, 1))
    attended = attend(queries, new_key, new_value, forget, kv_cache, cum_gates, lengths)
    head_part = jnp.dot(
        attended.reshape(row_count, heads_here * head_size),
        out_weight,
        preferred_element_type=jnp.float32,
    )
    slice_rows = row_count // lax.axis_size("tp")
    slice_start = lax.axis_index("tp") * slice_rows
    head_slice = summed_on_arrival(head_part.astype(jnp.bfloat16), "tp", 0)
    own_stream = lax.dynamic_slice_in_dim(layer_in, slice_start, slice_rows, 0)
    middle_slice = (own_stream.astype(jnp.float32) + head_slice).astype(jnp.bfloat16)
    hidden_slice = rms_scale(middle_slice, ffn_gain)
    middle, hidden_in = in_one_piece((middle_slice, hidden_slice), "tp", 0, 1)
    shared_hidden = (
        jax.nn.silu(jnp.dot(hidden_in, shared_gate, preferred_element_type=jnp.float32))
        * jnp.dot(hidden_in, shared_up, preferred_element_type=jnp.float32)
    ).astype(jnp.bfloat16)
    shared_part = jnp.dot(shared_hidden, shared_down, preferred_element_type=jnp.float32)
    my_gate = expert_gate[0]
    my_up = expert_up[0]
    my_down = expert_down[0]
    ep_count = lax.axis_size("ep")
    pair_count = lax.axis_size("tp") // 2
    column = lax.axis_index("tp") // 2
    picks = route_ids.shape[1]
    experts = ep_count * pair_count
    capacity = max(2, 4 * row_count * picks // (3 * experts))
    targets = jnp.arange(ep_count, dtype=jnp.int32) * pair_count + column
    matches = route_ids[:, :, None] == targets[None, None, :]
    member = jnp.any(matches, axis=1).astype(jnp.int32)
    weight = jnp.sum(jnp.where(matches, route_weights[:, :, None], 0.0), axis=1)
    ranking = jnp.cumsum(member, axis=0) - member
    slot_numbers = jnp.arange(capacity, dtype=jnp.int32)
    placement = (member[:, :, None] == 1) & (ranking[:, :, None] == slot_numbers[None, None, :])
    dispatch = jnp.einsum(
        "rs,rd->sd",
        placement.reshape(row_count, ep_count * capacity).astype(jnp.bfloat16),
        hidden_in,
        preferred_element_type=jnp.float32,
    ).astype(jnp.bfloat16)
    dispatch = dispatch.reshape(ep_count, capacity, width)
    received = lax.all_to_all(dispatch, "ep", split_axis=0, concat_axis=0, tiled=True)
    count = received.shape[1]
    batch_rows = received.reshape(ep_count * count, width)
    hidden = (
        jax.nn.silu(jnp.dot(batch_rows, my_gate, preferred_element_type=jnp.float32))
        * jnp.dot(batch_rows, my_up, preferred_element_type=jnp.float32)
    ).astype(jnp.bfloat16)
    served = jnp.dot(hidden, my_down, preferred_element_type=jnp.float32).reshape(
        ep_count, count, width
    )
    returned = lax.all_to_all(
        served.astype(jnp.bfloat16), "ep", split_axis=0, concat_axis=0, tiled=True
    ).astype(served.dtype)
    shares = (placement.astype(jnp.float32) * weight[:, :, None]).reshape(
        row_count, ep_count * capacity
    )
    routed = jnp.dot(
        shares,
        returned.reshape(ep_count * capacity, width),
        precision=lax.Precision.HIGHEST,
        preferred_element_type=jnp.float32,
    )
    mixed_slice = summed_on_arrival((shared_part + routed).astype(jnp.bfloat16), "tp", 0)
    own_middle = lax.dynamic_slice_in_dim(middle, slice_start, slice_rows, 0)
    out_slice = (own_middle.astype(jnp.float32) + mixed_slice).astype(jnp.bfloat16)
    layer_out = lax.all_gather(out_slice, "tp", axis=0, tiled=True)
    return (layer_out, new_kv)


def solution(mesh):
    placed = (
        P("ep", None),
        P(),
        P(None, "tp"),
        P(None, "tp"),
        P(None, "tp"),
        P(),
        P(),
        P("tp", None),
        P("ep", "tp", None, None),
        P("ep", "tp", None),
        P("ep"),
        P(),
        P("ep", None),
        P("ep", None),
        P(None, "tp"),
        P(None, "tp"),
        P("tp", None),
        P(("ep", "tp"), None, None),
        P(("ep", "tp"), None, None),
        P(("ep", "tp"), None, None),
    )
    return jax.shard_map(
        body,
        mesh=mesh,
        in_specs=placed,
        out_specs=(P("ep", None), P("ep", "tp", None)),
        check_vma=False,
    )
```

profile of v0, /device:TPU:1, one launch (start us, length us, event | category | flops | bytes accessed | tf_op | source)
XLA Modules:
  0.0 121.0 jit_solution(8280109137043809349)
XLA Ops:
  0.7 1.1 fusion.13
  1.9 0.7 broadcast_add_fusion
  2.5 1.1 fusion.55
  3.7 1.3 %convolution_convert_fusion.5 = bf16[32,64]{1,0:T(8,128)(2,1)S(1)} fusion(bf16[2048,64]{0,1:T(8,128)(2,1)} %param.22, bf16[32,2048]{1,0:T(8,128)(2,1)} %param.20, f32[2048]{0:T(1024)} %param.21, f32[32]{0:T(128)S(1)} %add_rsqrt_fusion.1), kind=kOutput, calls=%fused_computation.18 | convolution fusion | flops 8652800 | bytes 405632 | tf_op jit(solution)/shard_map/dot_general | solution.py:36
  5.0 1.4 %dynamic-slice = f32[1]{0:T(128)} dynamic-slice(f32[16]{0:T(128)} %param.26, s32[]{:T(128)S(6)} %select_n.30), dynamic_slice_sizes={1} | dynamic-slice | bytes 12 | tf_op jit(solution)/shard_map/dynamic_slice | solution.py:101
  6.4 1.8 %fusion.21 = f32[32]{0:T(128)S(1)} fusion(f32[32,1,1024]{2,1,0:T(1,128)} %param.29, s32[32]{0:T(128)S(1)} %broadcast_add_fusion), kind=kLoop, calls=%fused_computation.39 | loop fusion | flops 98272 | bytes 131328 | tf_op jit(solution)/shard_map/reduce_sum | solution.py:45
  8.1 5.6 %fusion.2 = f32[32,1,1024]{2,1,0:T(1,128)S(1)} fusion(bf16[32,1,1024,128]{3,2,1,0:T(8,128)(2,1)} %param.28, bf16[32,64,1]{1,0,2:T(8,128)(2,1)S(1)} %bitcast.54), kind=kOutput, calls=%fused_computation.2 | convolution fusion | flops 4194304 | bytes 8523776 | tf_op jit(solution)/shard_map/shd,shld->shl/dot_general | solution.py:50
  13.8 0.7 fusion.50
  14.6 0.1 fusion.17
  14.7 0.5 fusion.59
  15.2 1.0 multiply_reduce_fusion
  16.2 0.5 fusion.58
  16.8 2.6 %fusion = f32[32,1,64]{2,1,0:T(1,128)S(1)} fusion(bf16[32,1,1024,128]{3,2,1,0:T(8,128)(2,1)S(1)} %copy-done.1, f32[32]{0:T(128)S(1)} %get-tuple-element.9, f32[32,1,1024]{2,1,0:T(1,128)S(1)} %get-tuple-element.5, f32[32]{0:T(128)S(1)} %multiply_maximum_fusion), kind=kOutput, calls=%fused_computation | convolution fusion | flops 4292608 | bytes 8528128 | tf_op jit(solution)/shard_map/shl,shld->shd/dot_general | solution.py:61
  19.4 0.3 convolution_convert_fusion.3
  19.7 0.2 convolution_convert_fusion.2
  19.9 0.8 reshape.219
  20.7 10.0 %all-to-all-start = ((bf16[16,2,2048]{2,1,0:T(2,128)(2,1)}), bf16[16,2,2048]{2,1,0:T(2,128)(2,1)S(1)}, u32[]{:S(2)}, u32[]{:S(2)}) async-start(bf16[16,2,2048]{2,1,0:T(2,128)(2,1)} %reshape.219), calls=%async_computation | async-start | bytes 262144 | tf_op jit(solution)/shard_map/all_to_all | solution.py:16
  30.7 0.1 copy.39
  31.1 0.6 and.22
  31.7 0.7 eq.79
  32.4 0.7 fusion.28
  33.1 6.5 %all-to-all-done = bf16[16,2,2048]{2,1,0:T(2,128)(2,1)S(1)} async-done(((bf16[16,2,2048]{2,1,0:T(2,128)(2,1)}), bf16[16,2,2048]{2,1,0:T(2,128)(2,1)S(1)}, u32[]{:S(2)}, u32[]{:S(2)}) %all-to-all-start) | async-done | bytes 131104 | tf_op jit(solution)/shard_map/all_to_all | solution.py:16
  39.5 0.1 convert_reduce_fusion.1
  39.6 0.1 fusion.29
  39.9 16.6 %all-gather = bf16[16,2,4096]{2,1,0:T(2,128)(2,1)} all-gather(bf16[1,2,4096]{2,1,0:T(2,128)(2,1)S(1)} %maximum_bitcast_fusion), channel_id=1, replica_groups=mesh['ep'=16,'tp'=16] {'tp'}, dimensions={0}, use_global_device_ids=true | all-gather | bytes 278528 | tf_op jit(solution)/shard_map/all_gather | solution.py:22
  56.5 1.0 reshape.226
  57.5 0.9 convolution_convert_fusion.1
  58.5 0.8 reshape.220
  59.2 6.8 %all-to-all-start.1 = ((bf16[16,2,2048]{2,1,0:T(2,128)(2,1)}), bf16[16,2,2048]{2,1,0:T(2,128)(2,1)}, u32[]{:S(2)}, u32[]{:S(2)}) async-start(bf16[16,2,2048]{2,1,0:T(2,128)(2,1)} %reshape.220), calls=%async_computation.1 | async-start | bytes 262144 | tf_op jit(solution)/shard_map/all_to_all | solution.py:143
  66.0 1.3 %and_select_fusion = f32[32,16,2]{0,2,1:T(2,128)} fusion(pred[32,16]{0,1:T(8,128)(4,1)} %copy-done.7, f32[32,16]{0,1:T(8,128)} %fusion.28, s32[32,16]{0,1:T(8,128)S(1)} %copy.41), kind=kLoop, calls=%fused_computation.48 | loop fusion | flops 3072 | bytes 8704 | tf_op jit(solution)/shard_map/mul | solution.py:156
  67.4 5.6 %all-to-all-done.1 = bf16[16,2,2048]{2,1,0:T(2,128)(2,1)} async-done(((bf16[16,2,2048]{2,1,0:T(2,128)(2,1)}), bf16[16,2,2048]{2,1,0:T(2,128)(2,1)}, u32[]{:S(2)}, u32[]{:S(2)}) %all-to-all-start.1) | async-done | bytes 131104 | tf_op jit(solution)/shard_map/all_to_all | solution.py:143
  72.9 1.0 reshape.221
  73.9 0.3 fusion.11
  74.2 0.3 fusion.7
  74.5 0.3 convolution_convert_fusion
  74.8 0.8 copy.43
  75.6 3.5 %all-to-all-start.2 = ((bf16[16,2,2048]{2,1,0:T(2,128)(2,1)}), bf16[16,2,2048]{2,1,0:T(2,128)(2,1)S(1)}, u32[]{:S(2)}, u32[]{:S(2)}) async-start(bf16[16,2,2048]{2,1,0:T(2,128)(2,1)} %copy.43), calls=%async_computation.2 | async-start | bytes 262144 | tf_op jit(solution)/shard_map/all_to_all | solution.py:153
  79.1 1.1 fusion.25
  80.2 5.7 %all-to-all-done.2 = bf16[16,2,2048]{2,1,0:T(2,128)(2,1)S(1)} async-done(((bf16[16,2,2048]{2,1,0:T(2,128)(2,1)}), bf16[16,2,2048]{2,1,0:T(2,128)(2,1)S(1)}, u32[]{:S(2)}, u32[]{:S(2)}) %all-to-all-start.2) | async-done | bytes 131104 | tf_op jit(solution)/shard_map/all_to_all | solution.py:153
  85.9 1.0 convolution_bitcast_fusion
  87.0 1.3 %fusion.6 = bf16[32,2048]{1,0:T(8,128)(2,1)S(1)} fusion(f32[32,2048]{1,0:T(8,128)S(1)} %convolution_bitcast_fusion, bf16[32,2048]{1,0:T(8,128)(2,1)} %param.36, bf16[2048,32]{0,1:T(8,128)(2,1)} %param.35, bf16[32,4096]{1,0:T(8,128)(2,1)S(1)} %reshape.226, f32[32,32]{1,0:T(8,128)S(1)} %fusion.25), kind=kOutput, calls=%fused_computation.8 | convolution fusion | flops 8525824 | bytes 802816 | tf_op jit(solution)/shard_map/dot_general | solution.py:119
  88.3 0.8 reshape.222
  89.1 7.4 %all-to-all-start.3 = ((bf16[16,2,2048]{2,1,0:T(2,128)(2,1)}), bf16[16,2,2048]{2,1,0:T(2,128)(2,1)S(1)}, u32[]{:S(2)}, u32[]{:S(2)}) async-start(bf16[16,2,2048]{2,1,0:T(2,128)(2,1)} %reshape.222), calls=%async_computation.3 | async-start | bytes 262144 | tf_op jit(solution)/shard_map/all_to_all | solution.py:16
  96.5 1.4 %pad_maximum_fusion = bf16[32,1,128]{2,0,1:T(8,128)(2,1)} fusion(bf16[32,1,64]{2,0,1:T(8,128)(2,1)S(1)} %bitcast.55, bf16[32,1,64]{2,0,1:T(8,128)(2,1)} %bitcast.57), kind=kLoop, calls=%fused_computation.72 | loop fusion | flops 16384 | bytes 16384 | tf_op jit(solution)/shard_map/concatenate | solution.py:98
  97.9 7.5 %all-to-all-done.3 = bf16[16,2,2048]{2,1,0:T(2,128)(2,1)S(1)} async-done(((bf16[16,2,2048]{2,1,0:T(2,128)(2,1)}), bf16[16,2,2048]{2,1,0:T(2,128)(2,1)S(1)}, u32[]{:S(2)}, u32[]{:S(2)}) %all-to-all-start.3) | async-done | bytes 131104 | tf_op jit(solution)/shard_map/all_to_all | solution.py:16
  105.4 0.1 convert_reduce_fusion
  105.5 14.8 %all-gather.1 = bf16[16,2,2048]{2,1,0:T(2,128)(2,1)S(1)} all-gather(bf16[1,2,2048]{2,1,0:T(2,128)(2,1)S(1)} %fusion.42), channel_id=1, replica_groups=mesh['ep'=16,'tp'=16] {'tp'}, dimensions={0}, use_global_device_ids=true | all-gather | bytes 139264 | tf_op jit(solution)/shard_map/all_gather | solution.py:168
  120.3 0.7 reshape.228
  (49 shorter events, 0.6 us)
Async XLA Ops:
  0.6 73.9 %copy-start = (bf16[1,256,2048]{2,1,0:T(8,128)(2,1)S(1)}, bf16[1,256,2048]{2,1,0:T(8,128)(2,1)}, u32[]{:S(2)}) copy-start(bf16[1,256,2048]{2,1,0:T(8,128)(2,1)} %param.39) | copy-start | bytes 3145732
  0.6 14.6 %copy-start.6 = (bf16[32,2048]{1,0:T(8,128)(2,1)S(1)}, bf16[32,2048]{1,0:T(8,128)(2,1)}, u32[]{:S(2)}) copy-start(bf16[32,2048]{1,0:T(8,128)(2,1)} %param.20) | copy-start | bytes 393220
  0.7 14.0 %copy-start.11 = (s32[32]{0:T(128)S(1)}, s32[32]{0:T(128)}, u32[]{:S(2)}) copy-start(s32[32]{0:T(128)} %param.30) | copy-start | bytes 388
  0.7 14.5 %copy-start.14 = (f32[2048]{0:T(1024)S(1)}, f32[2048]{0:T(1024)}, u32[]{:S(2)}) copy-start(f32[2048]{0:T(1024)} %param.21) | copy-start | bytes 24580
  0.7 14.0 %copy-start.4 = (f32[32,1,1024]{2,1,0:T(1,128)S(1)}, f32[32,1,1024]{2,1,0:T(1,128)}, u32[]{:S(2)}) copy-start(f32[32,1,1024]{2,1,0:T(1,128)} %param.29) | copy-start | bytes 393220
  0.7 14.5 %copy-start.12 = (bf16[2048,64]{0,1:T(8,128)(2,1)S(1)}, bf16[2048,64]{0,1:T(8,128)(2,1)}, u32[]{:S(2)}) copy-start(bf16[2048,64]{0,1:T(8,128)(2,1)} %param.23) | copy-start | bytes 786436
  5.0 11.8 %copy-start.1 = (bf16[32,1,1024,128]{3,2,1,0:T(8,128)(2,1)S(1)}, bf16[32,1,1024,128]{3,2,1,0:T(8,128)(2,1)}, u32[]{:S(2)}) copy-start(bf16[32,1,1024,128]{3,2,1,0:T(8,128)(2,1)} %param.28) | copy-start | bytes 25165828
  13.8 5.6 %copy-start.13 = (bf16[2048,64]{0,1:T(8,128)(2,1)S(1)}, bf16[2048,64]{0,1:T(8,128)(2,1)}, u32[]{:S(2)}) copy-start(bf16[2048,64]{0,1:T(8,128)(2,1)} %param.24) | copy-start | bytes 786436
  13.8 5.9 %copy-start.5 = (bf16[64,2048]{1,0:T(8,128)(2,1)S(1)}, bf16[64,2048]{1,0:T(8,128)(2,1)}, u32[]{:S(2)}) copy-start(bf16[64,2048]{1,0:T(8,128)(2,1)} %param.27) | copy-start | bytes 786436
  13.8 16.9 %copy-start.8 = (s32[32,6]{0,1:T(8,128)S(1)}, s32[32,6]{0,1:T(8,128)}, u32[]{:S(2)}) copy-start(s32[32,6]{0,1:T(8,128)} %param.32) | copy-start | bytes 2308
  13.8 18.6 %copy-start.10 = (f32[32,6]{0,1:T(8,128)S(1)}, f32[32,6]{0,1:T(8,128)}, u32[]{:S(2)}) copy-start(f32[32,6]{0,1:T(8,128)} %param.33) | copy-start | bytes 2308
  13.8 26.0 %copy-start.9 = (f32[2048]{0:T(1024)S(1)}, f32[2048]{0:T(1024)}, u32[]{:S(2)}) copy-start(f32[2048]{0:T(1024)} %param.31) | copy-start | bytes 24580
  15.2 58.7 %copy-start.2 = (bf16[1,2048,256]{2,1,0:T(8,128)(2,1)S(1)}, bf16[1,2048,256]{2,1,0:T(8,128)(2,1)}, u32[]{:S(2)}) copy-start(bf16[1,2048,256]{2,1,0:T(8,128)(2,1)} %param.37) | copy-start | bytes 3145732
  16.8 57.4 %copy-start.3 = (bf16[1,2048,256]{2,1,0:T(8,128)(2,1)S(1)}, bf16[1,2048,256]{2,1,0:T(8,128)(2,1)}, u32[]{:S(2)}) copy-start(bf16[1,2048,256]{2,1,0:T(8,128)(2,1)} %param.38) | copy-start | bytes 3145732
  20.7 18.9 %all-to-all-start = ((bf16[16,2,2048]{2,1,0:T(2,128)(2,1)}), bf16[16,2,2048]{2,1,0:T(2,128)(2,1)S(1)}, u32[]{:S(2)}, u32[]{:S(2)}) async-start(bf16[16,2,2048]{2,1,0:T(2,128)(2,1)} %reshape.219), calls=%async_computation | async-start | bytes 262144 | tf_op jit(solution)/shard_map/all_to_all | solution.py:16
  31.1 2.0 %copy-start.7 = (pred[32,16]{0,1:T(8,128)(4,1)}, pred[32,16]{0,1:T(8,128)(4,1)S(1)}, u32[]{:S(2)}) copy-start(pred[32,16]{0,1:T(8,128)(4,1)S(1)} %copy.40) | copy-start | bytes 1540
  59.2 13.7 %all-to-all-start.1 = ((bf16[16,2,2048]{2,1,0:T(2,128)(2,1)}), bf16[16,2,2048]{2,1,0:T(2,128)(2,1)}, u32[]{:S(2)}, u32[]{:S(2)}) async-start(bf16[16,2,2048]{2,1,0:T(2,128)(2,1)} %reshape.220), calls=%async_computation.1 | async-start | bytes 262144 | tf_op jit(solution)/shard_map/all_to_all | solution.py:143
  75.6 10.3 %all-to-all-start.2 = ((bf16[16,2,2048]{2,1,0:T(2,128)(2,1)}), bf16[16,2,2048]{2,1,0:T(2,128)(2,1)S(1)}, u32[]{:S(2)}, u32[]{:S(2)}) async-start(bf16[16,2,2048]{2,1,0:T(2,128)(2,1)} %copy.43), calls=%async_computation.2 | async-start | bytes 262144 | tf_op jit(solution)/shard_map/all_to_all | solution.py:153
  89.1 16.3 %all-to-all-start.3 = ((bf16[16,2,2048]{2,1,0:T(2,128)(2,1)}), bf16[16,2,2048]{2,1,0:T(2,128)(2,1)S(1)}, u32[]{:S(2)}, u32[]{:S(2)}) async-start(bf16[16,2,2048]{2,1,0:T(2,128)(2,1)} %reshape.222), calls=%async_computation.3 | async-start | bytes 262144 | tf_op jit(solution)/shard_map/all_to_all | solution.py:16
where the time goes:
time: 122 us; the launch traced here: 121 us
  blocking collectives  31.4 us (26%)
  starting transfers between devices  27.7 us (23%)
  waiting for transfers between devices  25.3 us (21%)
  matrix products  17.3 us (14%)
  other arithmetic  9.49 us (8%)
  local copies, waits for them, and re-layouts  8.9 us (7%)
    all_to_all x2, starting transfers between devices, summed_on_arrival(): lax.all_to_all(tiles, axis, split_axis=0, concat_axis=0, tiled=True)  17.4 us
    all_gather x1, blocking collectives, in_one_piece(): filled, at, outs = (lax.all_gather(both, axis, axis=dim, tiled=True), 0, [])  16.6 us
    all_gather x1, blocking collectives, body(): layer_out = lax.all_gather(out_slice, 'tp', axis=0, tiled=True)  14.8 us
    all_to_all x2, waiting for transfers between devices, summed_on_arrival(): lax.all_to_all(tiles, axis, split_axis=0, concat_axis=0, tiled=True)  14 us
    all_to_all x1, starting transfers between devices, body(): lax.all_to_all(dispatch, 'ep', split_axis=0, concat_axis=0, tiled=True)  6.8 us
    all_to_all x1, waiting for transfers between devices, body(): lax.all_to_all(served.astype(jnp.bfloat16), 'ep', split_axis=0, concat_ax...  5.74 us
    dot_general x1, matrix products, attend(): jnp.einsum('shd,shld->shl', queries, cached_keys, preferred_element_type=...  5.63 us
    all_to_all x1, waiting for transfers between devices, body(): lax.all_to_all(dispatch, 'ep', split_axis=0, concat_axis=0, tiled=True)  5.58 us
  transfers between devices with their start and end apart: 4, of which 4 were waited for; matrix products, arithmetic and copies ran while one was open for 5% of the time, Pallas kernels for 0%

commit v1 on v0

--- a/solution.py
+++ b/solution.py
@@ -4,6 +4,18 @@
 from jax.sharding import PartitionSpec as P
 
 NORM_EPS = 1e-06
+
+
+def doubled_up(value, axis, dim):
+    ways, here, step = (lax.axis_size(axis), lax.axis_index(axis), value.shape[dim])
+    line, have = (value, 1)
+    while have < ways:
+        line = jnp.concatenate(
+            [line, lax.ppermute(line, axis, [(d, (d - have) % ways) for d in range(ways)])],
+            axis=dim,
+        )
+        have = 2 * have
+    return jnp.roll(line, here * step, axis=dim)
 
 
 def cut_along(shard, dim, peers):
@@ -165,7 +177,7 @@
     mixed_slice = summed_on_arrival((shared_part + routed).astype(jnp.bfloat16), "tp", 0)
     own_middle = lax.dynamic_slice_in_dim(middle, slice_start, slice_rows, 0)
     out_slice = (own_middle.astype(jnp.float32) + mixed_slice).astype(jnp.bfloat16)
-    layer_out = lax.all_gather(out_slice, "tp", axis=0, tiled=True)
+    layer_out = doubled_up(out_slice, "tp", 0)
     return (layer_out, new_kv)
 
 

time: 122 us -> 125 us (1.025)
  blocking collectives: 31.4 us -> 16.6 us
  waiting for transfers between devices: 25.3 us -> 35.8 us
  starting transfers between devices: 27.7 us -> 33.8 us
    all_gather x1 -> x0, blocking collectives: 14.8 us -> none  [body(): layer_out = lax.all_gather(out_slice, 'tp', axis=0, tiled=True)]
    ppermute x0 -> x4, waiting for transfers between devices: none -> 9.18 us  [doubled_up(): lax.ppermute(line, axis, [(d, (d - have) % ways) for d in range(ways)])]
    ppermute x0 -> x4, starting transfers between devices: none -> 6.11 us  [doubled_up(): lax.ppermute(line, axis, [(d, (d - have) % ways) for d in range(ways)])]
    all_to_all x2, waiting for transfers between devices: 14 us -> 15.3 us  [summed_on_arrival(): lax.all_to_all(tiles, axis, split_axis=0, concat_axis=0, tiled=True)]
  transfers between devices with their start and end apart: 4 -> 8, of which waited for: 4 -> 8; matrix products, arithmetic and copies ran while one was open for 5% -> 5% of each run, Pallas kernels for 0% -> 0%
where the time goes in v1:
time: 125 us; the launch traced here: 123 us
  waiting for transfers between devices  35.8 us (29%)
  starting transfers between devices  33.8 us (27%)
  matrix products  17.3 us (14%)
  blocking collectives  16.6 us (13%)
  other arithmetic  9.6 us (8%)
  local copies, waits for them, and re-layouts  8.99 us (7%)
    all_to_all x2, starting transfers between devices, summed_on_arrival(): lax.all_to_all(tiles, axis, split_axis=0, concat_axis=0, tiled=True)  17.4 us
    all_gather x1, blocking collectives, in_one_piece(): filled, at, outs = (lax.all_gather(both, axis, axis=dim, tiled=True), 0, [])  16.6 us
    all_to_all x2, waiting for transfers between devices, summed_on_arrival(): lax.all_to_all(tiles, axis, split_axis=0, concat_axis=0, tiled=True)  15.3 us
    ppermute x4, waiting for transfers between devices, doubled_up(): lax.ppermute(line, axis, [(d, (d - have) % ways) for d in range(ways)])  9.18 us
    all_to_all x1, starting transfers between devices, body(): lax.all_to_all(dispatch, 'ep', split_axis=0, concat_axis=0, tiled=True)  6.8 us
    ppermute x4, starting transfers between devices, doubled_up(): lax.ppermute(line, axis, [(d, (d - have) % ways) for d in range(ways)])  6.11 us
    all_to_all x1, waiting for transfers between devices, body(): lax.all_to_all(served.astype(jnp.bfloat16), 'ep', split_axis=0, concat_ax...  5.75 us
    dot_general x1, matrix products, attend(): jnp.einsum('shd,shld->shl', queries, cached_keys, preferred_element_type=...  5.63 us
  transfers between devices with their start and end apart: 8, of which 8 were waited for; matrix products, arithmetic and copies ran while one was open for 5% of the time, Pallas kernels for 0%

profile of v1, /device:TPU:1, one launch (start us, length us, event | category | flops | bytes accessed | tf_op | source)
XLA Modules:
  0.0 123.1 jit_solution(7583507851891789798)
XLA Ops:
  0.7 1.1 fusion.13
  1.9 0.7 broadcast_add_fusion
  2.5 1.1 fusion.54
  3.7 1.3 %convolution_convert_fusion.5 = bf16[32,64]{1,0:T(8,128)(2,1)S(1)} fusion(bf16[2048,64]{0,1:T(8,128)(2,1)} %param.22, bf16[32,2048]{1,0:T(8,128)(2,1)} %param.20, f32[2048]{0:T(1024)} %param.21, f32[32]{0:T(128)S(1)} %add_rsqrt_fusion.1), kind=kOutput, calls=%fused_computation.18 | convolution fusion | flops 8652800 | bytes 405632 | tf_op jit(solution)/shard_map/dot_general | solution.py:48
  5.0 1.4 %dynamic-slice = f32[1]{0:T(128)} dynamic-slice(f32[16]{0:T(128)} %param.26, s32[]{:T(128)S(6)} %select_n.42), dynamic_slice_sizes={1} | dynamic-slice | bytes 12 | tf_op jit(solution)/shard_map/dynamic_slice | solution.py:113
  6.4 1.8 %fusion.21 = f32[32]{0:T(128)S(1)} fusion(f32[32,1,1024]{2,1,0:T(1,128)} %param.29, s32[32]{0:T(128)S(1)} %broadcast_add_fusion), kind=kLoop, calls=%fused_computation.39 | loop fusion | flops 98272 | bytes 131328 | tf_op jit(solution)/shard_map/reduce_sum | solution.py:57
  8.1 5.6 %fusion.2 = f32[32,1,1024]{2,1,0:T(1,128)S(1)} fusion(bf16[32,1,1024,128]{3,2,1,0:T(8,128)(2,1)} %param.28, bf16[32,64,1]{1,0,2:T(8,128)(2,1)S(1)} %bitcast.52), kind=kOutput, calls=%fused_computation.2 | convolution fusion | flops 4194304 | bytes 8523776 | tf_op jit(solution)/shard_map/shd,shld->shl/dot_general | solution.py:62
  13.8 0.7 fusion.49
  14.7 0.5 fusion.58
  15.2 1.0 multiply_reduce_fusion
  16.2 0.5 fusion.57
  16.8 2.6 %fusion = f32[32,1,64]{2,1,0:T(1,128)S(1)} fusion(bf16[32,1,1024,128]{3,2,1,0:T(8,128)(2,1)S(1)} %copy-done.1, f32[32]{0:T(128)S(1)} %get-tuple-element.9, f32[32,1,1024]{2,1,0:T(1,128)S(1)} %get-tuple-element.5, f32[32]{0:T(128)S(1)} %multiply_maximum_fusion), kind=kOutput, calls=%fused_computation | convolution fusion | flops 4292608 | bytes 8528128 | tf_op jit(solution)/shard_map/shl,shld->shd/dot_general | solution.py:73
  19.4 0.3 convolution_convert_fusion.3
  19.9 0.8 reshape.219
  20.7 10.0 %all-to-all-start = ((bf16[16,2,2048]{2,1,0:T(2,128)(2,1)}), bf16[16,2,2048]{2,1,0:T(2,128)(2,1)S(1)}, u32[]{:S(2)}, u32[]{:S(2)}) async-start(bf16[16,2,2048]{2,1,0:T(2,128)(2,1)} %reshape.219), calls=%async_computation | async-start | bytes 262144 | tf_op jit(solution)/shard_map/all_to_all | solution.py:28
  31.1 0.6 and.28
  31.7 0.7 eq.82
  32.4 0.7 fusion.28
  33.1 6.5 %all-to-all-done = bf16[16,2,2048]{2,1,0:T(2,128)(2,1)S(1)} async-done(((bf16[16,2,2048]{2,1,0:T(2,128)(2,1)}), bf16[16,2,2048]{2,1,0:T(2,128)(2,1)S(1)}, u32[]{:S(2)}, u32[]{:S(2)}) %all-to-all-start) | async-done | bytes 131104 | tf_op jit(solution)/shard_map/all_to_all | solution.py:28
  39.9 16.6 %all-gather = bf16[16,2,4096]{2,1,0:T(2,128)(2,1)} all-gather(bf16[1,2,4096]{2,1,0:T(2,128)(2,1)S(1)} %maximum_bitcast_fusion), channel_id=1, replica_groups=mesh['ep'=16,'tp'=16] {'tp'}, dimensions={0}, use_global_device_ids=true | all-gather | bytes 278528 | tf_op jit(solution)/shard_map/all_gather | solution.py:34
  56.5 1.0 reshape.226
  57.5 0.9 convolution_convert_fusion.1
  58.5 0.8 reshape.220
  59.2 6.8 %all-to-all-start.1 = ((bf16[16,2,2048]{2,1,0:T(2,128)(2,1)}), bf16[16,2,2048]{2,1,0:T(2,128)(2,1)}, u32[]{:S(2)}, u32[]{:S(2)}) async-start(bf16[16,2,2048]{2,1,0:T(2,128)(2,1)} %reshape.220), calls=%async_computation.1 | async-start | bytes 262144 | tf_op jit(solution)/shard_map/all_to_all | solution.py:155
  66.0 1.3 %and_select_fusion = f32[32,16,2]{0,2,1:T(2,128)} fusion(pred[32,16]{0,1:T(8,128)(4,1)} %copy-done.7, f32[32,16]{0,1:T(8,128)} %fusion.28, s32[32,16]{0,1:T(8,128)S(1)} %copy.41), kind=kLoop, calls=%fused_computation.50 | loop fusion | flops 3072 | bytes 8704 | tf_op jit(solution)/shard_map/mul | solution.py:168
  67.4 5.6 %all-to-all-done.1 = bf16[16,2,2048]{2,1,0:T(2,128)(2,1)} async-done(((bf16[16,2,2048]{2,1,0:T(2,128)(2,1)}), bf16[16,2,2048]{2,1,0:T(2,128)(2,1)}, u32[]{:S(2)}, u32[]{:S(2)}) %all-to-all-start.1) | async-done | bytes 131104 | tf_op jit(solution)/shard_map/all_to_all | solution.py:155
  72.9 1.0 reshape.221
  73.9 0.3 fusion.11
  74.2 0.3 fusion.7
  74.5 0.3 convolution_convert_fusion
  74.8 0.8 copy.43
  75.6 3.5 %all-to-all-start.2 = ((bf16[16,2,2048]{2,1,0:T(2,128)(2,1)}), bf16[16,2,2048]{2,1,0:T(2,128)(2,1)S(1)}, u32[]{:S(2)}, u32[]{:S(2)}) async-start(bf16[16,2,2048]{2,1,0:T(2,128)(2,1)} %copy.43), calls=%async_computation.2 | async-start | bytes 262144 | tf_op jit(solution)/shard_map/all_to_all | solution.py:165
  79.1 1.1 fusion.25
  80.2 5.7 %all-to-all-done.2 = bf16[16,2,2048]{2,1,0:T(2,128)(2,1)S(1)} async-done(((bf16[16,2,2048]{2,1,0:T(2,128)(2,1)}), bf16[16,2,2048]{2,1,0:T(2,128)(2,1)S(1)}, u32[]{:S(2)}, u32[]{:S(2)}) %all-to-all-start.2) | async-done | bytes 131104 | tf_op jit(solution)/shard_map/all_to_all | solution.py:165
  85.9 1.0 convolution_bitcast_fusion
  87.0 1.3 %fusion.6 = bf16[32,2048]{1,0:T(8,128)(2,1)S(1)} fusion(f32[32,2048]{1,0:T(8,128)S(1)} %convolution_bitcast_fusion, bf16[32,2048]{1,0:T(8,128)(2,1)} %param.36, bf16[2048,32]{0,1:T(8,128)(2,1)} %param.35, bf16[32,4096]{1,0:T(8,128)(2,1)S(1)} %reshape.226, f32[32,32]{1,0:T(8,128)S(1)} %fusion.25), kind=kOutput, calls=%fused_computation.8 | convolution fusion | flops 8525824 | bytes 802816 | tf_op jit(solution)/shard_map/dot_general | solution.py:131
  88.3 0.8 reshape.222
  89.1 7.4 %all-to-all-start.3 = ((bf16[16,2,2048]{2,1,0:T(2,128)(2,1)}), bf16[16,2,2048]{2,1,0:T(2,128)(2,1)S(1)}, u32[]{:S(2)}, u32[]{:S(2)}) async-start(bf16[16,2,2048]{2,1,0:T(2,128)(2,1)} %reshape.222), calls=%async_computation.3 | async-start | bytes 262144 | tf_op jit(solution)/shard_map/all_to_all | solution.py:28
  96.5 8.9 %all-to-all-done.3 = bf16[16,2,2048]{2,1,0:T(2,128)(2,1)S(1)} async-done(((bf16[16,2,2048]{2,1,0:T(2,128)(2,1)}), bf16[16,2,2048]{2,1,0:T(2,128)(2,1)S(1)}, u32[]{:S(2)}, u32[]{:S(2)}) %all-to-all-start.3) | async-done | bytes 131104 | tf_op jit(solution)/shard_map/all_to_all | solution.py:28
  105.5 3.1 %collective-permute-done = bf16[2,2048]{1,0:T(2,128)(2,1)S(1)} collective-permute-done((bf16[2,2048]{1,0:T(2,128)(2,1)S(1)}, bf16[2,2048]{1,0:T(2,128)(2,1)S(1)}, u32[]{:S(2)}, u32[]{:S(2)}) %collective-permute-start) | collective-permute-done | bytes 8224 | tf_op jit(solution)/shard_map/ppermute | solution.py:14
  108.6 1.3 %collective-permute-start.1 = (bf16[4,2048]{1,0:T(4,128)(2,1)S(1)}, bf16[4,2048]{1,0:T(4,128)(2,1)S(1)}, u32[]{:S(2)}, u32[]{:S(2)}) collective-permute-start(bf16[4,2048]{1,0:T(4,128)(2,1)S(1)} %pad_maximum_fusion.2), channel_id=1, source_target_pairs={{0,14},{1,15},{2,0},{3,1},{4,2},{5,3},{6,4},{7,5},{8,6},{9,7},{10,... | collective-permute-start | bytes 49160 | tf_op jit(solution)/shard_map/ppermute | solution.py:14
  110.0 1.3 %collective-permute-done.1 = bf16[4,2048]{1,0:T(4,128)(2,1)S(1)} collective-permute-done((bf16[4,2048]{1,0:T(4,128)(2,1)S(1)}, bf16[4,2048]{1,0:T(4,128)(2,1)S(1)}, u32[]{:S(2)}, u32[]{:S(2)}) %collective-permute-start.1) | collective-permute-done | bytes 16416 | tf_op jit(solution)/shard_map/ppermute | solution.py:14
  111.3 1.1 collective-permute-start.2
  112.4 2.7 %collective-permute-done.2 = bf16[8,2048]{1,0:T(8,128)(2,1)S(1)} collective-permute-done((bf16[8,2048]{1,0:T(8,128)(2,1)S(1)}, bf16[8,2048]{1,0:T(8,128)(2,1)S(1)}, u32[]{:S(2)}, u32[]{:S(2)}) %collective-permute-start.2) | collective-permute-done | bytes 32800 | tf_op jit(solution)/shard_map/ppermute | solution.py:14
  115.1 3.7 %collective-permute-start.3 = (bf16[16,2048]{1,0:T(8,128)(2,1)S(1)}, bf16[16,2048]{1,0:T(8,128)(2,1)S(1)}, u32[]{:S(2)}, u32[]{:S(2)}) collective-permute-start(bf16[16,2048]{1,0:T(8,128)(2,1)S(1)} %pad_maximum_fusion), channel_id=1, source_target_pairs={{0,8},{1,9},{2,10},{3,11},{4,12},{5,13},{6,14},{7,15},{8,0},{9,1},... | collective-permute-start | bytes 196616 | tf_op jit(solution)/shard_map/ppermute | solution.py:14
  118.8 1.4 %pad_maximum_fusion.3 = bf16[32,1,128]{2,0,1:T(8,128)(2,1)} fusion(bf16[32,1,64]{2,0,1:T(8,128)(2,1)S(1)} %bitcast.53, bf16[32,1,64]{2,0,1:T(8,128)(2,1)} %bitcast.55), kind=kLoop, calls=%fused_computation.74 | loop fusion | flops 16384 | bytes 16384 | tf_op jit(solution)/shard_map/concatenate | solution.py:110
  120.2 2.1 %collective-permute-done.3 = bf16[16,2048]{1,0:T(8,128)(2,1)S(1)} collective-permute-done((bf16[16,2048]{1,0:T(8,128)(2,1)S(1)}, bf16[16,2048]{1,0:T(8,128)(2,1)S(1)}, u32[]{:S(2)}, u32[]{:S(2)}) %collective-permute-start.3) | collective-permute-done | bytes 65568 | tf_op jit(solution)/shard_map/ppermute | solution.py:14
  122.4 0.7 constant_dynamic-slice_fusion
  (60 shorter events, 1.6 us)
Async XLA Ops:
  0.6 73.9 %copy-start = (bf16[1,256,2048]{2,1,0:T(8,128)(2,1)S(1)}, bf16[1,256,2048]{2,1,0:T(8,128)(2,1)}, u32[]{:S(2)}) copy-start(bf16[1,256,2048]{2,1,0:T(8,128)(2,1)} %param.39) | copy-start | bytes 3145732
  0.6 14.6 %copy-start.6 = (bf16[32,2048]{1,0:T(8,128)(2,1)S(1)}, bf16[32,2048]{1,0:T(8,128)(2,1)}, u32[]{:S(2)}) copy-start(bf16[32,2048]{1,0:T(8,128)(2,1)} %param.20) | copy-start | bytes 393220
  0.7 14.0 %copy-start.11 = (s32[32]{0:T(128)S(1)}, s32[32]{0:T(128)}, u32[]{:S(2)}) copy-start(s32[32]{0:T(128)} %param.30) | copy-start | bytes 388
  0.7 14.5 %copy-start.14 = (f32[2048]{0:T(1024)S(1)}, f32[2048]{0:T(1024)}, u32[]{:S(2)}) copy-start(f32[2048]{0:T(1024)} %param.21) | copy-start | bytes 24580
  0.7 14.0 %copy-start.4 = (f32[32,1,1024]{2,1,0:T(1,128)S(1)}, f32[32,1,1024]{2,1,0:T(1,128)}, u32[]{:S(2)}) copy-start(f32[32,1,1024]{2,1,0:T(1,128)} %param.29) | copy-start | bytes 393220
  0.7 14.5 %copy-start.12 = (bf16[2048,64]{0,1:T(8,128)(2,1)S(1)}, bf16[2048,64]{0,1:T(8,128)(2,1)}, u32[]{:S(2)}) copy-start(bf16[2048,64]{0,1:T(8,128)(2,1)} %param.23) | copy-start | bytes 786436
  5.0 11.8 %copy-start.1 = (bf16[32,1,1024,128]{3,2,1,0:T(8,128)(2,1)S(1)}, bf16[32,1,1024,128]{3,2,1,0:T(8,128)(2,1)}, u32[]{:S(2)}) copy-start(bf16[32,1,1024,128]{3,2,1,0:T(8,128)(2,1)} %param.28) | copy-start | bytes 25165828
  13.8 5.6 %copy-start.13 = (bf16[2048,64]{0,1:T(8,128)(2,1)S(1)}, bf16[2048,64]{0,1:T(8,128)(2,1)}, u32[]{:S(2)}) copy-start(bf16[2048,64]{0,1:T(8,128)(2,1)} %param.24) | copy-start | bytes 786436
  13.8 5.9 %copy-start.5 = (bf16[64,2048]{1,0:T(8,128)(2,1)S(1)}, bf16[64,2048]{1,0:T(8,128)(2,1)}, u32[]{:S(2)}) copy-start(bf16[64,2048]{1,0:T(8,128)(2,1)} %param.27) | copy-start | bytes 786436
  13.8 16.9 %copy-start.8 = (s32[32,6]{0,1:T(8,128)S(1)}, s32[32,6]{0,1:T(8,128)}, u32[]{:S(2)}) copy-start(s32[32,6]{0,1:T(8,128)} %param.32) | copy-start | bytes 2308
  13.8 18.6 %copy-start.10 = (f32[32,6]{0,1:T(8,128)S(1)}, f32[32,6]{0,1:T(8,128)}, u32[]{:S(2)}) copy-start(f32[32,6]{0,1:T(8,128)} %param.33) | copy-start | bytes 2308
  13.8 26.0 %copy-start.9 = (f32[2048]{0:T(1024)S(1)}, f32[2048]{0:T(1024)}, u32[]{:S(2)}) copy-start(f32[2048]{0:T(1024)} %param.31) | copy-start | bytes 24580
  15.2 58.7 %copy-start.2 = (bf16[1,2048,256]{2,1,0:T(8,128)(2,1)S(1)}, bf16[1,2048,256]{2,1,0:T(8,128)(2,1)}, u32[]{:S(2)}) copy-start(bf16[1,2048,256]{2,1,0:T(8,128)(2,1)} %param.37) | copy-start | bytes 3145732
  16.8 57.4 %copy-start.3 = (bf16[1,2048,256]{2,1,0:T(8,128)(2,1)S(1)}, bf16[1,2048,256]{2,1,0:T(8,128)(2,1)}, u32[]{:S(2)}) copy-start(bf16[1,2048,256]{2,1,0:T(8,128)(2,1)} %param.38) | copy-start | bytes 3145732
  20.7 18.9 %all-to-all-start = ((bf16[16,2,2048]{2,1,0:T(2,128)(2,1)}), bf16[16,2,2048]{2,1,0:T(2,128)(2,1)S(1)}, u32[]{:S(2)}, u32[]{:S(2)}) async-start(bf16[16,2,2048]{2,1,0:T(2,128)(2,1)} %reshape.219), calls=%async_computation | async-start | bytes 262144 | tf_op jit(solution)/shard_map/all_to_all | solution.py:28
  31.1 2.0 %copy-start.7 = (pred[32,16]{0,1:T(8,128)(4,1)}, pred[32,16]{0,1:T(8,128)(4,1)S(1)}, u32[]{:S(2)}) copy-start(pred[32,16]{0,1:T(8,128)(4,1)S(1)} %copy.40) | copy-start | bytes 1540
  59.2 13.7 %all-to-all-start.1 = ((bf16[16,2,2048]{2,1,0:T(2,128)(2,1)}), bf16[16,2,2048]{2,1,0:T(2,128)(2,1)}, u32[]{:S(2)}, u32[]{:S(2)}) async-start(bf16[16,2,2048]{2,1,0:T(2,128)(2,1)} %reshape.220), calls=%async_computation.1 | async-start | bytes 262144 | tf_op jit(solution)/shard_map/all_to_all | solution.py:155
  75.6 10.3 %all-to-all-start.2 = ((bf16[16,2,2048]{2,1,0:T(2,128)(2,1)}), bf16[16,2,2048]{2,1,0:T(2,128)(2,1)S(1)}, u32[]{:S(2)}, u32[]{:S(2)}) async-start(bf16[16,2,2048]{2,1,0:T(2,128)(2,1)} %copy.43), calls=%async_computation.2 | async-start | bytes 262144 | tf_op jit(solution)/shard_map/all_to_all | solution.py:165
  89.1 16.3 %all-to-all-start.3 = ((bf16[16,2,2048]{2,1,0:T(2,128)(2,1)}), bf16[16,2,2048]{2,1,0:T(2,128)(2,1)S(1)}, u32[]{:S(2)}, u32[]{:S(2)}) async-start(bf16[16,2,2048]{2,1,0:T(2,128)(2,1)} %reshape.222), calls=%async_computation.3 | async-start | bytes 262144 | tf_op jit(solution)/shard_map/all_to_all | solution.py:28
  105.5 3.1 %collective-permute-start = (bf16[2,2048]{1,0:T(2,128)(2,1)S(1)}, bf16[2,2048]{1,0:T(2,128)(2,1)S(1)}, u32[]{:S(2)}, u32[]{:S(2)}) collective-permute-start(bf16[2,2048]{1,0:T(2,128)(2,1)S(1)} %add_convert_fusion), channel_id=1, source_target_pairs={{0,15},{1,0},{2,1},{3,2},{4,3},{5,4},{6,5},{7,6},{8,7},{9,8},{10,9... | collective-permute-start | bytes 24584 | tf_op jit(solution)/shard_map/ppermute | solution.py:14
  108.6 2.7 %collective-permute-start.1 = (bf16[4,2048]{1,0:T(4,128)(2,1)S(1)}, bf16[4,2048]{1,0:T(4,128)(2,1)S(1)}, u32[]{:S(2)}, u32[]{:S(2)}) collective-permute-start(bf16[4,2048]{1,0:T(4,128)(2,1)S(1)} %pad_maximum_fusion.2), channel_id=1, source_target_pairs={{0,14},{1,15},{2,0},{3,1},{4,2},{5,3},{6,4},{7,5},{8,6},{9,7},{10,... | collective-permute-start | bytes 49160 | tf_op jit(solution)/shard_map/ppermute | solution.py:14
  111.3 3.7 %collective-permute-start.2 = (bf16[8,2048]{1,0:T(8,128)(2,1)S(1)}, bf16[8,2048]{1,0:T(8,128)(2,1)S(1)}, u32[]{:S(2)}, u32[]{:S(2)}) collective-permute-start(bf16[8,2048]{1,0:T(8,128)(2,1)S(1)} %pad_maximum_fusion.1), channel_id=1, source_target_pairs={{0,12},{1,13},{2,14},{3,15},{4,0},{5,1},{6,2},{7,3},{8,4},{9,5},{1... | collective-permute-start | bytes 98312 | tf_op jit(solution)/shard_map/ppermute | solution.py:14
  115.1 7.2 %collective-permute-start.3 = (bf16[16,2048]{1,0:T(8,128)(2,1)S(1)}, bf16[16,2048]{1,0:T(8,128)(2,1)S(1)}, u32[]{:S(2)}, u32[]{:S(2)}) collective-permute-start(bf16[16,2048]{1,0:T(8,128)(2,1)S(1)} %pad_maximum_fusion), channel_id=1, source_target_pairs={{0,8},{1,9},{2,10},{3,11},{4,12},{5,13},{6,14},{7,15},{8,0},{9,1},... | collective-permute-start | bytes 196616 | tf_op jit(solution)/shard_map/ppermute | solution.py:14
